TPU v7x, 32 devices: a whole 2x2x4 slice. The times are simulated.
32 devices in a mesh: sp: 4 (over y, x), tp: 8 (over z, core).
Axes of the slice: x: 2, y: 2, z: 4, core: 2. Of those that a mesh axis runs over, the one named last changes fastest.
Arguments:
- tokens: bfloat16 [3, 2048, 4096], P(None, 'sp', 'tp'), may hold values from -6 to 6
- new_token: bfloat16 [3, 1, 4096], P(None, None, 'tp'), may hold values from -6 to 6
- query_weight: bfloat16 [4096, 4096], P(None, 'tp'), may hold values from -0.09375 to 0.09375
- key_weight: bfloat16 [4096, 4096], P(None, 'tp'), may hold values from -0.09375 to 0.09375
- value_weight: bfloat16 [4096, 4096], P(None, 'tp'), may hold values from -0.09375 to 0.09375
- log_decay: float32 [64], P('tp'), may hold values from -0.034 to 0
Outputs:
- state: bfloat16 [3, 64, 64, 64], P(None, 'tp', 'sp')
- read: bfloat16 [3, 4096], P(None, 'tp')
All inputs are finite; a program needn't handle non-finite values.
Results may differ from a plain program's by a relative error of at most 0.012.
Values may be sent and summed in bfloat16 or wider, within the bound.
A program may use at most 64 MiB of HBM per device.

v0:
```python
import jax
import jax.numpy as jnp
from jax import lax
from jax.sharding import PartitionSpec as P

HD = 64


def rotate(values, positions):
    half_dim = values.shape[-1] // 2
    inverse = 10000.0 ** (-jnp.arange(half_dim, dtype=jnp.float32) / half_dim)
    angles = positions.astype(jnp.float32)[:, None, None] * inverse[None, None, :]
    cosine = jnp.cos(angles)
    sine_part = jnp.sin(angles)
    first = values[..., :half_dim]
    second = values[..., half_dim:]
    return jnp.concatenate(
        [first * cosine - second * sine_part, first * sine_part + second * cosine], axis=-1
    )


def group_norm(output):
    centered = output - jnp.mean(output, axis=-1, keepdims=True)
    return centered * lax.rsqrt(jnp.mean(centered * centered, axis=-1, keepdims=True) + 1e-05)


def body(tokens, new_token, query_weight, key_weight, value_weight, log_decay):
    sequences, span_len, _ = tokens.shape
    head_count = log_decay.shape[0]
    inner = head_count * HD
    groups = lax.axis_size("sp")
    own_index = lax.axis_index("sp")
    key_scale = HD ** (-0.5)
    key_share = HD // groups
    row_weights = jnp.concatenate([key_weight, value_weight], axis=1)
    all_weights = jnp.concatenate([key_weight, value_weight, query_weight], axis=1)
    row_piece = lax.all_gather(tokens, "tp", axis=2, tiled=True)
    new_piece = lax.all_gather(new_token, "tp", axis=2, tiled=True)
    row_total = jnp.dot(row_piece, row_weights, preferred_element_type=jnp.float32)
    new_total = jnp.dot(new_piece, all_weights, preferred_element_type=jnp.float32)
    row_total = row_total.reshape(sequences, span_len, 2, head_count, HD)
    offsets = own_index * span_len + jnp.arange(span_len, dtype=jnp.int32)
    key_rows = (rotate(row_total[:, :, 0], offsets) * key_scale).astype(jnp.bfloat16)
    value_rows = row_total[:, :, 1].astype(jnp.bfloat16)
    to_end = (span_len - 1 - jnp.arange(span_len, dtype=jnp.int32)).astype(jnp.float32)
    decay_rows = jnp.exp(to_end[:, None] * log_decay[None, :])
    weighted = (key_rows.astype(jnp.float32) * decay_rows[None, :, :, None]).astype(jnp.bfloat16)
    span_state = jnp.einsum(
        "sthk,sthv->shkv", weighted, value_rows, preferred_element_type=jnp.float32
    )
    carried_state = jnp.exp(log_decay * (span_len * (groups - 1 - own_index)).astype(jnp.float32))
    scaled_state = span_state * carried_state[None, :, None, None]
    state_rows = lax.psum_scatter(scaled_state, "sp", scatter_dimension=2, tiled=True)
    new_total = new_total.reshape(sequences, 1, 3, head_count, HD)
    new_position = jnp.full((1,), groups * span_len, jnp.int32)
    fresh_key = (rotate(new_total[:, :, 0], new_position) * key_scale).astype(jnp.bfloat16)[:, 0]
    new_value = new_total[:, 0, 1].astype(jnp.bfloat16)
    new_query = rotate(new_total[:, :, 2], new_position).astype(jnp.bfloat16)[:, 0]
    query_entries = new_query.astype(jnp.float32)
    decay_one = jnp.exp(log_decay)[None, :, None]
    query_share = lax.dynamic_slice_in_dim(query_entries, own_index * key_share, key_share, 2)
    partial_read = (
        jnp.einsum("shkv,shk->shv", state_rows, query_share, precision=lax.Precision.HIGHEST)
        * decay_one
    )
    summed = lax.psum(partial_read, "sp")
    own_term = jnp.sum(
        query_entries * fresh_key.astype(jnp.float32), axis=-1, keepdims=True
    ) * new_value.astype(jnp.float32)
    normed = group_norm(summed + own_term)
    return (state_rows.astype(jnp.bfloat16), normed.reshape(sequences, inner).astype(jnp.bfloat16))


def solution(mesh):
    return jax.shard_map(
        body,
        mesh=mesh,
        in_specs=(
            P(None, "sp", "tp"),
            P(None, None, "tp"),
            P(None, "tp"),
            P(None, "tp"),
            P(None, "tp"),
            P("tp"),
        ),
        out_specs=(P(None, "tp", "sp", None), P(None, "tp")),
        check_vma=False,
    )
```

profile of v0, /device:TPU:0, one launch (start us, length us, event | category | flops | bytes accessed | tf_op | source)
XLA Modules:
  0.0 200.9 jit_solution(10623617118696532471)
XLA Ops:
  7.2 0.0 all-gather.2.cloned.1.call-start
  7.2 0.7 all-gather.2.cloned.1.call-update
  7.9 0.0 reduce-scatter.2.cloned.1.call-start
  7.9 6.4 %copy.9 = bf16[4096,512]{0,1:T(8,128)(2,1)} copy(bf16[4096,512]{1,0:T(8,128)(2,1)} %param.10) | data formatting | bytes 8388608 | tf_op args[4]
  14.3 0.0 copy-start
  14.3 0.0 copy-start.1
  14.3 6.5 %copy.8 = bf16[4096,512]{0,1:T(8,128)(2,1)} copy(bf16[4096,512]{1,0:T(8,128)(2,1)} %param.9) | data formatting | bytes 8388608 | tf_op args[3]
  20.8 0.0 copy-done
  20.8 16.8 %all_gather.7 = bf16[3,1,4096]{2,0,1:T(4,128)(2,1)S(1)} all-gather(bf16[3,1,512]{2,0,1:T(4,128)(2,1)S(1)} %copy-done), channel_id=1, replica_groups=mesh['sp'=4,'tp'=8] {'tp'}, dimensions={2}, use_global_device_ids=true | all-gather | bytes 27648 | tf_op jit(solution)/shard_map/all_gather | solution.py:38
  37.7 0.0 copy-done.1
  37.7 0.1 multiply_exponential_fusion
  37.8 0.3 multiply_cosine_fusion
  38.1 91.1 %all-gather.2.cloned.1.call-done = bf16[3,512,4096]{2,1,0:T(8,128)(2,1)} async-done(((bf16[3,512,512]{2,1,0:T(8,128)(2,1)}), bf16[3,512,4096]{2,1,0:T(8,128)(2,1)}) %all-gather.2.cloned.1.call-update) | async-done | bytes 12582928 | tf_op jit(solution)/shard_map/all_gather | solution.py:37
  129.3 18.5 %fusion.7 = f32[1024,3,512]{2,0,1:T(8,128)S(1)} fusion(bf16[3,512,4096]{2,1,0:T(8,128)(2,1)} %all-gather.2.cloned.1.call-done, bf16[4096,512]{0,1:T(8,128)(2,1)} %copy.9, bf16[4096,512]{0,1:T(8,128)(2,1)} %copy.8), kind=kOutput, calls=%fused_computation.8 | convolution fusion | flops 12901679104 | bytes 27262976 | tf_op jit(solution)/shard_map/dot_general | solution.py:39
  147.8 0.3 copy_bitcast_fusion
  148.1 0.5 multiply_subtract_fusion
  148.5 1.5 fusion.20
  150.0 0.0 reduce-scatter.2.cloned.1.call-update
  150.0 5.6 %fusion.11 = f32[3,1536]{1,0:T(4,128)S(1)} fusion(bf16[4096,512]{1,0:T(8,128)(2,1)} %param.8, bf16[4096,512]{1,0:T(8,128)(2,1)} %param.10, bf16[4096,512]{1,0:T(8,128)(2,1)} %param.9, bf16[3,1,4096]{2,0,1:T(4,128)(2,1)S(1)} %all_gather.7), kind=kOutput, calls=%fused_computation.16 | convolution fusion | flops 75497472 | bytes 12625920 | tf_op jit(solution)/shard_map/dot_general | solution.py:40
  155.6 0.1 reshape.216
  155.7 0.1 multiply_sine_fusion.1
  155.8 0.1 subtract_bitcast_fusion
  155.8 0.1 fusion.31
  155.9 18.7 %reduce-scatter.2.cloned.1.call-done = f32[3,8,16,64]{3,2,1,0:T(8,128)} async-done(((f32[3,8,64,64]{3,2,1,0:T(8,128)}), f32[3,8,16,64]{3,2,1,0:T(8,128)}) %reduce-scatter.2.cloned.1.call-update) | async-done | bytes 98320 | tf_op jit(solution)/shard_map/reduce_scatter | solution.py:53
  174.6 1.1 fusion.27
  175.7 0.1 broadcast_multiply_fusion
  175.8 15.0 %psum.7 = f32[3,8,64]{2,1,0:T(8,128)S(1)} all-reduce(f32[3,8,64]{2,1,0:T(8,128)S(1)} %broadcast_multiply_fusion), channel_id=1, replica_groups=mesh['sp'=4,'tp'=8] {'sp'}, use_global_device_ids=true, to_apply=%region_1.0 | all-reduce | flops 1536 | bytes 12288 | tf_op jit(solution)/shard_map/psum | solution.py:66
  190.8 0.7 fusion.38
  191.6 0.2 multiply_reduce_fusion
  191.7 0.1 multiply_convert_fusion.4
  191.8 0.7 convert_element_type.83
  192.5 1.6 convert_element_type.76
  (7 shorter events, 0.0 us)
Async XLA Ops:
  7.2 122.1 %all-gather.2.cloned.1.call-start = ((), (), s32[]{:S(2)}) async-start(), calls=%async_computation.1 | async-start | bytes 14155776 | tf_op jit(solution)/shard_map/all_gather | solution.py:37
  7.9 166.7 %reduce-scatter.2.cloned.1.call-start = ((), (), s32[]{:S(2)}) async-start(), calls=%async_computation.2 | async-start | bytes 983040 | tf_op jit(solution)/shard_map/reduce_scatter | solution.py:53
  14.3 6.5 %copy-start = (bf16[3,1,512]{2,0,1:T(4,128)(2,1)S(1)}, bf16[3,1,512]{2,0,1:T(4,128)(2,1)}, u32[]{:S(2)}) copy-start(bf16[3,1,512]{2,0,1:T(4,128)(2,1)} %param.7) | copy-start | bytes 9220
  14.3 23.4 %copy-start.1 = (f32[8]{0:T(128)S(1)}, f32[8]{0:T(128)}, u32[]{:S(2)}) copy-start(f32[8]{0:T(128)} %param.11) | copy-start | bytes 100
Sparse Core Ops, SparseCore 0:
  9.6 119.6 all-gather.1
  150.1 24.4 reduce-scatter.1
where the time goes:
time: 201 us
  waiting for transfers between devices  110 us (55%)
  blocking collectives  31.9 us (16%)
  matrix products  26.7 us (13%)
  between operations  14.1 us (7%)
  local copies, waits for them, and re-layouts  14 us (7%)
  other arithmetic  3.69 us (2%)
    all_gather x1, waiting for transfers between devices, body(): row_piece = lax.all_gather(tokens, 'tp', axis=2, tiled=True)  91.1 us
    reduce_scatter x1, waiting for transfers between devices, body(): lax.psum_scatter(scaled_state, 'sp', scatter_dimension=2, tiled=True)  18.7 us
    dot_general x1, matrix products, body(): jnp.dot(row_piece, row_weights, preferred_element_type=jnp.float32)  18.5 us
    all_gather x1, blocking collectives, body(): new_piece = lax.all_gather(new_token, 'tp', axis=2, tiled=True)  16.8 us
    psum x1, blocking collectives, body(): summed = lax.psum(partial_read, 'sp')  15 us
    unnamed x6, local copies, waits for them, and re-layouts  12.9 us
    dot_general x1, matrix products, body(): jnp.dot(new_piece, all_weights, preferred_element_type=jnp.float32)  5.59 us
  transfers between devices with their start and end apart: 2, of which 2 were waited for; matrix products, arithmetic and copies ran while one was open for 10% of the time, Pallas kernels for 0%

commit v1 on v0

v1 whole, which is shorter than its diff:
```python
import functools

import jax
import jax.numpy as jnp
from jax import lax
from jax.experimental import pallas as pl
from jax.experimental.pallas import tpu as pltpu
from jax.sharding import PartitionSpec as P

HD = 64
LANES = 128
NEW_ROWS = 8
F32 = jnp.float32
BF16 = jnp.bfloat16


def lane_iota(shape):
    return lax.broadcasted_iota(jnp.int32, shape, len(shape) - 1)


def rotated(block, cosine, sine):
    half = HD // 2
    low = lane_iota(block.shape) % HD < half
    swapped = jnp.where(
        low, pltpu.roll(block, LANES - half, 1), pltpu.roll(block, half, 1)
    )
    return block * cosine + swapped * sine


def kernel(
    n_sp, n_tp,
    tokens, fresh, wq_hbm, wk_hbm, wv_hbm, inverse_ref, decay_ref,
    state_out, read_out,
    x, nx, wq, wk, wv, acc_k, acc_v, cos_ref, sin_ref, fade_ref, rows_ref,
    q_spread, own_term, stage, landed, totals,
    load_sem, weight_sem, rx, rn, fwd, share, nfwd, nshare, rs_tx, rs_rx,
):
    seqs, span, feat = tokens.shape
    inner = wk.shape[1]
    heads = inner // HD
    chips = n_tp // 2
    keep = HD // n_sp
    sp = lax.axis_index("sp")
    tp = lax.axis_index("tp")
    z, k = tp // 2, tp % 2
    MESH = pl.DeviceIdType.MESH

    def to_tp(index):
        return {"tp": index}

    partner = z * 2 + 1 - k
    own_loads = [
        pltpu.make_async_copy(tokens.at[s], x.at[tp, s], load_sem.at[s]) for s in range(seqs)
    ]
    new_load = pltpu.make_async_copy(fresh, nx.at[tp], load_sem.at[seqs])
    new_load.start()
    for copy in own_loads:
        copy.start()
    weight_loads = [
        pltpu.make_async_copy(a, b, weight_sem.at[i])
        for i, (a, b) in enumerate(((wk_hbm, wk), (wv_hbm, wv), (wq_hbm, wq)))
    ]
    for copy in weight_loads:
        copy.start()

    barrier = pltpu.get_barrier_semaphore()

    @pl.when(z > 0)
    def _():
        pl.semaphore_signal(barrier, inc=1, device_id=to_tp(tp - 2), device_id_type=MESH)

    @pl.when(z < chips - 1)
    def _():
        pl.semaphore_signal(barrier, inc=1, device_id=to_tp(tp + 2), device_id_type=MESH)

    pl.semaphore_signal(barrier, inc=1, device_id=to_tp(partner), device_id_type=MESH)
    for o in range(1, n_sp):
        pl.semaphore_signal(
            barrier, inc=1, device_id={"sp": lax.rem(sp + o, n_sp)}, device_id_type=MESH
        )
    pl.semaphore_wait(
        barrier, n_sp + (z > 0).astype(jnp.int32) + (z < chips - 1).astype(jnp.int32)
    )

    def x_copy(c, s, sem, target):
        p = 2 * c + k
        return pltpu.make_async_remote_copy(
            x.at[p, s], x.at[p, s], sem, rx.at[p, s], device_id=to_tp(target), device_id_type=MESH
        )

    def n_copy(c, sem, target):
        p = 2 * c + k
        return pltpu.make_async_remote_copy(
            nx.at[p], nx.at[p], sem, rn.at[p], device_id=to_tp(target), device_id_type=MESH
        )

    def x_arrived(p, s):
        pltpu.make_async_remote_copy(
            x.at[p, s], x.at[p, s], share.at[0, 0], rx.at[p, s],
            device_id=to_tp(partner), device_id_type=MESH,
        ).wait_recv()

    def n_arrived(p):
        pltpu.make_async_remote_copy(
            nx.at[p], nx.at[p], nshare.at[0], rn.at[p],
            device_id=to_tp(partner), device_id_type=MESH,
        ).wait_recv()

    new_load.wait()
    n_up = n_copy(z, nfwd.at[0, z], tp + 2)
    n_down = n_copy(z, nfwd.at[1, z], tp - 2)
    n_side = n_copy(z, nshare.at[z], partner)

    @pl.when(z < chips - 1)
    def _():
        n_up.start()

    @pl.when(z > 0)
    def _():
        n_down.start()

    n_side.start()
    for s in range(seqs):
        own_loads[s].wait()

        @pl.when(z < chips - 1)
        def _(s=s):
            x_copy(z, s, fwd.at[0, z, s], tp + 2).start()

        @pl.when(z > 0)
        def _(s=s):
            x_copy(z, s, fwd.at[1, z, s], tp - 2).start()

        x_copy(z, s, share.at[z, s], partner).start()

    row = lax.broadcasted_iota(jnp.int32, (span, LANES), 0)
    within = lane_iota((1, LANES)) % HD
    first_half = jnp.where(within < HD // 2, -1.0, 1.0).astype(F32)
    inverse = inverse_ref[...]
    angles = (sp * span + row).astype(F32) * inverse
    cos_ref[...] = jnp.cos(angles)
    sin_ref[...] = jnp.sin(angles) * first_half
    new_angles = jnp.full((NEW_ROWS, LANES), n_sp * span, F32) * inverse
    new_cos = jnp.cos(new_angles)
    new_sin = jnp.sin(new_angles) * first_half
    head_of = lane_iota((1, inner)) // HD
    rate = jnp.zeros((1, inner), F32)
    for h in range(heads):
        rate = jnp.where(head_of == h, decay_ref[h], rate)
    to_end = (span - 1 - lax.broadcasted_iota(jnp.int32, (span, 1), 0)).astype(F32)
    fade_ref[...] = jnp.exp(to_end * rate)
    rows_ref[0:1] = jnp.exp(rate * (span * (n_sp - 1 - sp)).astype(F32))
    rows_ref[1:2] = jnp.exp(rate)

    for copy in weight_loads:
        copy.wait()

    def add(p, s, fresh_total):
        block = x[p, s]
        where = pl.ds(pl.multiple_of(p * feat, feat), feat)
        part_k = jnp.dot(block, wk[where, :], preferred_element_type=F32)
        part_v = jnp.dot(block, wv[where, :], preferred_element_type=F32)
        if fresh_total:
            acc_k[s] = part_k
            acc_v[s] = part_v
        else:
            acc_k[s] += part_k
            acc_v[s] += part_v

    @pl.loop(0, seqs)
    def _(s):
        add(tp, s, True)
        x_arrived(partner, s)
        add(partner, s, False)

    n_arrived(partner)

    def project_new():
        def piece(p, totals):
            where = pl.ds(pl.multiple_of(p * feat, feat), feat)
            block = nx[p]
            return tuple(
                t + jnp.dot(block, w[where, :], preferred_element_type=F32)
                for t, w in zip(totals, (wk, wv, wq))
            )

        zero = jnp.zeros((NEW_ROWS, inner), F32)
        new_k, new_v, new_q = lax.fori_loop(0, n_tp, piece, (zero, zero, zero))
        keys, queries = [], []
        for j in range(inner // LANES):
            at = slice(j * LANES, (j + 1) * LANES)
            keys.append((rotated(new_k[:, at], new_cos, new_sin) * HD**-0.5).astype(BF16))
            queries.append(rotated(new_q[:, at], new_cos, new_sin).astype(BF16))
        key = jnp.concatenate(keys, axis=1).astype(F32)
        query = jnp.concatenate(queries, axis=1).astype(F32)
        value = new_v.astype(BF16).astype(F32)
        same = (
            lax.broadcasted_iota(jnp.int32, (inner, inner), 0) // HD
            == lax.broadcasted_iota(jnp.int32, (inner, inner), 1) // HD
        )
        product = query * key
        for h in range(heads):
            at = slice(h * HD, (h + 1) * HD)
            own_term[:, at] = jnp.sum(product[:, at], axis=-1, keepdims=True) * value[:, at]
        pick = lax.broadcasted_iota(jnp.int32, (HD, inner), 0) == lane_iota((HD, inner)) % HD
        for s in range(seqs):
            spread = jnp.where(pick, query[s : s + 1], 0.0).astype(BF16)
            q_spread[s] = jnp.dot(
                spread, jnp.where(same, 1.0, 0.0).astype(BF16), preferred_element_type=F32
            )

    def rs_copy(s, o):
        peer = lax.rem(sp + o, n_sp)
        return pltpu.make_async_remote_copy(
            stage.at[s, peer], landed.at[s, sp], rs_tx.at[s, peer], rs_rx.at[s, sp],
            device_id={"sp": peer}, device_id_type=MESH,
        )

    def finish(s):
        cosine, sine = cos_ref[...], sin_ref[...]
        lane = lane_iota((HD, LANES))
        for j in range(inner // LANES):
            at = slice(j * LANES, (j + 1) * LANES)
            key = (rotated(acc_k[s, :, at], cosine, sine) * HD**-0.5).astype(BF16)
            weighted = (key.astype(F32) * fade_ref[:, at]).astype(BF16)
            value = acc_v[s, :, at].astype(BF16)
            both = lax.dot_general(
                weighted, value, (((0,), (0,)), ((), ())), preferred_element_type=F32
            )
            state = jnp.where(lane < HD, both[:HD], both[HD:]) * rows_ref[0:1, at]
            part = jnp.sum(state * q_spread[s, :, at], axis=0, keepdims=True)
            for o in range(n_sp):
                stage[s, o, 0:keep, at] = state[o * keep : (o + 1) * keep]
                stage[s, o, keep : keep + 1, at] = part
        for o in range(1, n_sp):
            rs_copy(s, o).start()
        landed_own = stage[s, sp]
        totals[s] = landed_own

    far = jnp.maximum(z, chips - 1 - z)

    def decode(i):
        d = i // (2 * seqs) + 1
        s = (i // 2) % seqs
        step = 2 * (i % 2) - 1
        c = z + step * d
        return d, s, step, c, (c >= 0) & (c < chips)

    def onward(step):
        nxt = z - step
        return nxt, (nxt >= 0) & (nxt < chips), (step + 1) // 2

    @pl.loop(0, 2 * seqs * (chips - 1))
    def _(i):
        d, s, step, c, valid = decode(i)
        nxt, pass_on, way = onward(step)

        @pl.when(valid)
        def _():
            @pl.when(s == 0)
            def _():
                n_arrived(2 * c + k)

                @pl.when(pass_on)
                def _():
                    n_copy(c, nfwd.at[way, c], 2 * nxt + k).start()

                n_copy(c, nshare.at[c], partner).start()

            x_arrived(2 * c + k, s)

            @pl.when(pass_on)
            def _():
                x_copy(c, s, fwd.at[way, c, s], 2 * nxt + k).start()

            x_copy(c, s, share.at[c, s], partner).start()
            add(2 * c + k, s, False)

            @pl.when(s == 0)
            def _():
                n_arrived(2 * c + 1 - k)

            x_arrived(2 * c + 1 - k, s)
            add(2 * c + 1 - k, s, False)

        last = (d == far) & (step == 1)

        @pl.when(last & (s == 0))
        def _():
            project_new()

        @pl.when(last)
        def _():
            finish(s)

    raws = []
    for s in range(seqs):
        for o in range(1, n_sp):
            src = lax.rem(sp + o, n_sp)
            pltpu.make_async_remote_copy(
                stage.at[s, src], landed.at[s, src], rs_tx.at[s, src], rs_rx.at[s, src],
                device_id={"sp": src}, device_id_type=MESH,
            ).wait_recv()
        total = None
        for j in range(n_sp):
            term = jnp.where(sp == j, totals[s], landed[s, j])
            total = term if total is None else total + term
        kept = total[0:keep].astype(BF16)
        for h in range(heads):
            state_out[s, h] = kept[:, h * HD : (h + 1) * HD]
        raws.append(total[keep : keep + 1] * rows_ref[1:2] + own_term[s : s + 1])
    raw = jnp.concatenate(raws, axis=0)
    for h in range(heads):
        at = slice(h * HD, (h + 1) * HD)
        head = raw[:, at]
        centered = head - jnp.mean(head, axis=-1, keepdims=True)
        spread = jnp.mean(centered * centered, axis=-1, keepdims=True)
        read_out[:, at] = (centered * lax.rsqrt(spread + 1e-05)).astype(BF16)

    @pl.when(z < chips - 1)
    def _():
        n_up.wait_send()

    @pl.when(z > 0)
    def _():
        n_down.wait_send()

    n_side.wait_send()
    for s in range(seqs):
        @pl.when(z < chips - 1)
        def _(s=s):
            x_copy(z, s, fwd.at[0, z, s], tp + 2).wait_send()

        @pl.when(z > 0)
        def _(s=s):
            x_copy(z, s, fwd.at[1, z, s], tp - 2).wait_send()

        x_copy(z, s, share.at[z, s], partner).wait_send()
        for o in range(1, n_sp):
            rs_copy(s, o).wait_send()

    @pl.loop(0, 2 * seqs * (chips - 1))
    def _(i):
        d, s, step, c, valid = decode(i)
        nxt, pass_on, way = onward(step)

        @pl.when(valid)
        def _():
            @pl.when(s == 0)
            def _():
                @pl.when(pass_on)
                def _():
                    n_copy(c, nfwd.at[way, c], 2 * nxt + k).wait_send()

                n_copy(c, nshare.at[c], partner).wait_send()

            @pl.when(pass_on)
            def _():
                x_copy(c, s, fwd.at[way, c, s], 2 * nxt + k).wait_send()

            x_copy(c, s, share.at[c, s], partner).wait_send()


def solution(mesh):
    n_sp, n_tp = mesh.shape["sp"], mesh.shape["tp"]

    def body(tokens, new_token, query_weight, key_weight, value_weight, log_decay):
        seqs, span, feat = tokens.shape
        width, inner = key_weight.shape
        heads = inner // HD
        keep = HD // n_sp
        rows = -(-(keep + 1) // 8) * 8
        chips = n_tp // 2
        half = HD // 2
        inverse = 10000.0 ** (-jnp.arange(half, dtype=F32) / half)
        inverse = jnp.tile(inverse, LANES // half)[None]
        fresh = jnp.pad(new_token[:, 0], ((0, NEW_ROWS - seqs), (0, 0)))
        anywhere = pl.BlockSpec(memory_space=pl.ANY)
        vmem = pl.BlockSpec(memory_space=pltpu.VMEM)
        dma = pltpu.SemaphoreType.DMA
        return pl.pallas_call(
            functools.partial(kernel, n_sp, n_tp),
            out_shape=(
                jax.ShapeDtypeStruct((seqs, heads, keep, HD), BF16),
                jax.ShapeDtypeStruct((seqs, inner), BF16),
            ),
            in_specs=[anywhere] * 5 + [vmem, pl.BlockSpec(memory_space=pltpu.SMEM)],
            out_specs=(vmem, vmem),
            scratch_shapes=[
                pltpu.VMEM((n_tp, seqs, span, feat), BF16),
                pltpu.VMEM((n_tp, NEW_ROWS, feat), BF16),
                pltpu.VMEM((width, inner), BF16),
                pltpu.VMEM((width, inner), BF16),
                pltpu.VMEM((width, inner), BF16),
                pltpu.VMEM((seqs, span, inner), F32),
                pltpu.VMEM((seqs, span, inner), F32),
                pltpu.VMEM((span, LANES), F32),
                pltpu.VMEM((span, LANES), F32),
                pltpu.VMEM((span, inner), F32),
                pltpu.VMEM((8, inner), F32),
                pltpu.VMEM((seqs, HD, inner), F32),
                pltpu.VMEM((NEW_ROWS, inner), F32),
                pltpu.VMEM((seqs, n_sp, rows, inner), F32),
                pltpu.VMEM((seqs, n_sp, rows, inner), F32),
                pltpu.VMEM((seqs, rows, inner), F32),
                dma((seqs + 1,)),
                dma((3,)),
                dma((n_tp, seqs)),
                dma((n_tp,)),
                dma((2, chips, seqs)),
                dma((chips, seqs)),
                dma((2, chips)),
                dma((chips,)),
                dma((seqs, n_sp)),
                dma((seqs, n_sp)),
            ],
            compiler_params=pltpu.CompilerParams(
                collective_id=0, has_side_effects=True, vmem_limit_bytes=60 * 1024 * 1024
            ),
            name="retention",
        )(tokens, fresh, query_weight, key_weight, value_weight, inverse, log_decay)

    return jax.shard_map(
        body,
        mesh=mesh,
        in_specs=(
            P(None, "sp", "tp"),
            P(None, None, "tp"),
            P(None, "tp"),
            P(None, "tp"),
            P(None, "tp"),
            P("tp"),
        ),
        out_specs=(P(None, "tp", "sp", None), P(None, "tp")),
        check_vma=False,
    )
```

time: 201 us -> 124 us (0.62)
  Pallas kernels: 0 us -> 118 us
  waiting for transfers between devices: 110 us -> 0 us
  blocking collectives: 31.9 us -> 0 us
  matrix products: 26.7 us -> 0 us
  between operations: 14.1 us -> 0.65 us
  local copies, waits for them, and re-layouts: 14 us -> 4.7 us
  other arithmetic: 3.69 us -> 0.01 us
    pallas_call x0 -> x1, Pallas kernels: none -> 118 us  [body(): pl.pallas_call(functools.partial(kernel, n_sp, n_tp), out_shape=(jax.Shap...]
    all_gather x1 -> x0, waiting for transfers between devices: 91.1 us -> none  [body(): row_piece = lax.all_gather(tokens, 'tp', axis=2, tiled=True)]
    dot_general x4 -> x0, matrix products: 26.7 us -> none  [the longest x1 18.5 us: body(): jnp.dot(row_piece, row_weights, preferred_element_type=jnp.float32)]
    reduce_scatter x1 -> x0, waiting for transfers between devices: 18.7 us -> none  [body(): lax.psum_scatter(scaled_state, 'sp', scatter_dimension=2, tiled=True)]
    all_gather x1 -> x0, blocking collectives: 16.8 us -> none  [body(): new_piece = lax.all_gather(new_token, 'tp', axis=2, tiled=True)]
    psum x1 -> x0, blocking collectives: 15 us -> none  [body(): summed = lax.psum(partial_read, 'sp')]
    unnamed x6 -> x2, local copies, waits for them, and re-layouts: 12.9 us -> 2.82 us
  transfers between devices with their start and end apart: 2 -> 0, of which waited for: 2 -> 0; matrix products, arithmetic and copies ran while one was open for 10% -> 0% of each run, Pallas kernels for 0% -> 0%
where the time goes in v1:
time: 124 us
  Pallas kernels  118 us (95%)
  local copies, waits for them, and re-layouts  4.7 us (4%)
    pallas_call x1, Pallas kernels, body(): pl.pallas_call(functools.partial(kernel, n_sp, n_tp), out_shape=(jax.Shap...  118 us
    unnamed x2, local copies, waits for them, and re-layouts  2.82 us

profile of v1, /device:TPU:0, one launch (start us, length us, event | category | flops | bytes accessed | tf_op | source)
XLA Modules:
  0.0 123.6 jit_solution(13863460723366087571)
XLA Ops:
  0.7 0.6 broadcast_in_dim_tile.3.inverse_ref
  1.2 1.3 %pad.4.fresh = bf16[8,512]{1,0:T(8,128)(2,1)} pad(bf16[3,512]{1,0:T(4,128)(2,1)} %bitcast.1, bf16[]{:T(256)} %constant.2.clone.1), padding=0_5x0_0 | pad | bytes 11266 | tf_op jit(solution)/shard_map/jit(_pad)/pad | solution.py:377
  2.5 118.2 %retention.1 = (bf16[3,8,16,64]{3,2,1,0:T(8,128)(2,1)}, bf16[3,512]{1,0:T(4,128)(2,1)}) custom-call(bf16[3,512,512]{2,1,0:T(8,128)(2,1)} %tokens.1, bf16[8,512]{1,0:T(8,128)(2,1)} %pad.4.fresh, bf16[4096,512]{1,0:T(8,128)(2,1)} %wq_hbm.1, bf16[4096,512]{1,0:T(8,128)(2,1)} %wk_hbm.1, bf16[4096,512]{1,0:T(8,128)(2,1)} %wv_hbm.1, ...), custom_call_target="tpu_custom_call" | custom-call | tf_op jit(solution)/shard_map/retention/pallas_call | solution.py:381
  120.8 1.5 %copy.10 = bf16[3,8,16,64]{3,2,1,0:T(8,128)(2,1)} copy(bf16[3,8,16,64]{3,2,1,0:T(8,128)(2,1)} %get-tuple-element.4) | data formatting | bytes 98304
  122.3 1.3 %copy.11 = bf16[3,512]{1,0:T(4,128)(2,1)} copy(bf16[3,512]{1,0:T(4,128)(2,1)} %get-tuple-element.5) | data formatting | bytes 6144
  (2 shorter events, 0.0 us)

commit v2 on v1

--- a/solution.py
+++ b/solution.py
@@ -2,6 +2,7 @@
 
 import jax
 import jax.numpy as jnp
+import numpy as np
 from jax import lax
 from jax.experimental import pallas as pl
 from jax.experimental.pallas import tpu as pltpu
@@ -28,17 +29,19 @@
 
 
 def kernel(
-    n_sp, n_tp,
+    n_sp, n_tp, parts,
     tokens, fresh, wq_hbm, wk_hbm, wv_hbm, inverse_ref, decay_ref,
     state_out, read_out,
     x, nx, wq, wk, wv, acc_k, acc_v, cos_ref, sin_ref, fade_ref, rows_ref,
-    q_spread, own_term, stage, landed, totals,
+    q_spread, own_term, sums, stage, landed, totals,
     load_sem, weight_sem, rx, rn, fwd, share, nfwd, nshare, rs_tx, rs_rx,
 ):
     seqs, span, feat = tokens.shape
     inner = wk.shape[1]
     heads = inner // HD
     chips = n_tp // 2
+    pieces = seqs * parts
+    size = span // parts
     keep = HD // n_sp
     sp = lax.axis_index("sp")
     tp = lax.axis_index("tp")
@@ -50,9 +53,12 @@
 
     partner = z * 2 + 1 - k
     own_loads = [
-        pltpu.make_async_copy(tokens.at[s], x.at[tp, s], load_sem.at[s]) for s in range(seqs)
+        pltpu.make_async_copy(
+            tokens.at[s // parts, pl.ds(s % parts * size, size)], x.at[tp, s], load_sem.at[s]
+        )
+        for s in range(pieces)
     ]
-    new_load = pltpu.make_async_copy(fresh, nx.at[tp], load_sem.at[seqs])
+    new_load = pltpu.make_async_copy(fresh, nx.at[tp], load_sem.at[pieces])
     new_load.start()
     for copy in own_loads:
         copy.start()
@@ -60,8 +66,6 @@
         pltpu.make_async_copy(a, b, weight_sem.at[i])
         for i, (a, b) in enumerate(((wk_hbm, wk), (wv_hbm, wv), (wq_hbm, wq)))
     ]
-    for copy in weight_loads:
-        copy.start()
 
     barrier = pltpu.get_barrier_semaphore()
 
@@ -120,7 +124,7 @@
         n_down.start()
 
     n_side.start()
-    for s in range(seqs):
+    for s in range(pieces):
         own_loads[s].wait()
 
         @pl.when(z < chips - 1)
@@ -132,6 +136,9 @@
             x_copy(z, s, fwd.at[1, z, s], tp - 2).start()
 
         x_copy(z, s, share.at[z, s], partner).start()
+
+    for copy in weight_loads:
+        copy.start()
 
     row = lax.broadcasted_iota(jnp.int32, (span, LANES), 0)
     within = lane_iota((1, LANES)) % HD
@@ -167,7 +174,7 @@
             acc_k[s] += part_k
             acc_v[s] += part_v
 
-    @pl.loop(0, seqs)
+    @pl.loop(0, pieces)
     def _(s):
         add(tp, s, True)
         x_arrived(partner, s)
@@ -178,7 +185,9 @@
     def project_new():
         def piece(p, totals):
             where = pl.ds(pl.multiple_of(p * feat, feat), feat)
-            block = nx[p]
+            block = jnp.concatenate(
+                [nx[p].astype(F32), jnp.zeros((NEW_ROWS - seqs, feat), F32)], axis=0
+            ).astype(BF16)
             return tuple(
                 t + jnp.dot(block, w[where, :], preferred_element_type=F32)
                 for t, w in zip(totals, (wk, wv, wq))
@@ -216,32 +225,38 @@
             device_id={"sp": peer}, device_id_type=MESH,
         )
 
-    def finish(s):
-        cosine, sine = cos_ref[...], sin_ref[...]
+    def finish(i):
+        s, part = i // parts, i % parts
+        where = pl.ds(pl.multiple_of(part * size, size), size)
+        cosine, sine = cos_ref[where, :], sin_ref[where, :]
         lane = lane_iota((HD, LANES))
         for j in range(inner // LANES):
             at = slice(j * LANES, (j + 1) * LANES)
-            key = (rotated(acc_k[s, :, at], cosine, sine) * HD**-0.5).astype(BF16)
-            weighted = (key.astype(F32) * fade_ref[:, at]).astype(BF16)
-            value = acc_v[s, :, at].astype(BF16)
+            key = (rotated(acc_k[i, :, at], cosine, sine) * HD**-0.5).astype(BF16)
+            weighted = (key.astype(F32) * fade_ref[where, at]).astype(BF16)
+            value = acc_v[i, :, at].astype(BF16)
             both = lax.dot_general(
                 weighted, value, (((0,), (0,)), ((), ())), preferred_element_type=F32
             )
-            state = jnp.where(lane < HD, both[:HD], both[HD:]) * rows_ref[0:1, at]
-            part = jnp.sum(state * q_spread[s, :, at], axis=0, keepdims=True)
+            state = jnp.where(lane < HD, both[:HD], both[HD:])
+            sums[:, at] = jnp.where(part == 0, state, sums[:, at] + state)
+
+        @pl.when(part == parts - 1)
+        def _():
+            scaled = sums[...] * rows_ref[0:1]
+            read = jnp.sum(scaled * q_spread[s], axis=0, keepdims=True)
             for o in range(n_sp):
-                stage[s, o, 0:keep, at] = state[o * keep : (o + 1) * keep]
-                stage[s, o, keep : keep + 1, at] = part
-        for o in range(1, n_sp):
-            rs_copy(s, o).start()
-        landed_own = stage[s, sp]
-        totals[s] = landed_own
+                stage[s, o, 0:keep] = scaled[o * keep : (o + 1) * keep]
+                stage[s, o, keep : keep + 1] = read
+            for o in range(1, n_sp):
+                rs_copy(s, o).start()
+            totals[s] = stage[s, sp]
 
     far = jnp.maximum(z, chips - 1 - z)
 
     def decode(i):
-        d = i // (2 * seqs) + 1
-        s = (i // 2) % seqs
+        d = i // (2 * pieces) + 1
+        s = (i // 2) % pieces
         step = 2 * (i % 2) - 1
         c = z + step * d
         return d, s, step, c, (c >= 0) & (c < chips)
@@ -250,7 +265,7 @@
         nxt = z - step
         return nxt, (nxt >= 0) & (nxt < chips), (step + 1) // 2
 
-    @pl.loop(0, 2 * seqs * (chips - 1))
+    @pl.loop(0, 2 * pieces * (chips - 1))
     def _(i):
         d, s, step, c, valid = decode(i)
         nxt, pass_on, way = onward(step)
@@ -327,6 +342,9 @@
 
     n_side.wait_send()
     for s in range(seqs):
+        for o in range(1, n_sp):
+            rs_copy(s, o).wait_send()
+    for s in range(pieces):
         @pl.when(z < chips - 1)
         def _(s=s):
             x_copy(z, s, fwd.at[0, z, s], tp + 2).wait_send()
@@ -336,10 +354,8 @@
             x_copy(z, s, fwd.at[1, z, s], tp - 2).wait_send()
 
         x_copy(z, s, share.at[z, s], partner).wait_send()
-        for o in range(1, n_sp):
-            rs_copy(s, o).wait_send()
-
-    @pl.loop(0, 2 * seqs * (chips - 1))
+
+    @pl.loop(0, 2 * pieces * (chips - 1))
     def _(i):
         d, s, step, c, valid = decode(i)
         nxt, pass_on, way = onward(step)
@@ -372,14 +388,15 @@
         rows = -(-(keep + 1) // 8) * 8
         chips = n_tp // 2
         half = HD // 2
-        inverse = 10000.0 ** (-jnp.arange(half, dtype=F32) / half)
-        inverse = jnp.tile(inverse, LANES // half)[None]
-        fresh = jnp.pad(new_token[:, 0], ((0, NEW_ROWS - seqs), (0, 0)))
+        parts = max(1, 8 // chips)
+        pieces = seqs * parts
+        inverse = np.float32(10000.0) ** (-np.arange(half, dtype=np.float32) / half)
+        inverse = jnp.asarray(np.tile(inverse.astype(np.float32), LANES // half)[None])
         anywhere = pl.BlockSpec(memory_space=pl.ANY)
         vmem = pl.BlockSpec(memory_space=pltpu.VMEM)
         dma = pltpu.SemaphoreType.DMA
         return pl.pallas_call(
-            functools.partial(kernel, n_sp, n_tp),
+            functools.partial(kernel, n_sp, n_tp, parts),
             out_shape=(
                 jax.ShapeDtypeStruct((seqs, heads, keep, HD), BF16),
                 jax.ShapeDtypeStruct((seqs, inner), BF16),
@@ -387,28 +404,29 @@
             in_specs=[anywhere] * 5 + [vmem, pl.BlockSpec(memory_space=pltpu.SMEM)],
             out_specs=(vmem, vmem),
             scratch_shapes=[
-                pltpu.VMEM((n_tp, seqs, span, feat), BF16),
-                pltpu.VMEM((n_tp, NEW_ROWS, feat), BF16),
+                pltpu.VMEM((n_tp, pieces, span // parts, feat), BF16),
+                pltpu.VMEM((n_tp, seqs, feat), BF16),
                 pltpu.VMEM((width, inner), BF16),
                 pltpu.VMEM((width, inner), BF16),
                 pltpu.VMEM((width, inner), BF16),
-                pltpu.VMEM((seqs, span, inner), F32),
-                pltpu.VMEM((seqs, span, inner), F32),
+                pltpu.VMEM((pieces, span // parts, inner), F32),
+                pltpu.VMEM((pieces, span // parts, inner), F32),
                 pltpu.VMEM((span, LANES), F32),
                 pltpu.VMEM((span, LANES), F32),
                 pltpu.VMEM((span, inner), F32),
                 pltpu.VMEM((8, inner), F32),
                 pltpu.VMEM((seqs, HD, inner), F32),
                 pltpu.VMEM((NEW_ROWS, inner), F32),
+                pltpu.VMEM((HD, inner), F32),
                 pltpu.VMEM((seqs, n_sp, rows, inner), F32),
                 pltpu.VMEM((seqs, n_sp, rows, inner), F32),
                 pltpu.VMEM((seqs, rows, inner), F32),
-                dma((seqs + 1,)),
+                dma((pieces + 1,)),
                 dma((3,)),
-                dma((n_tp, seqs)),
+                dma((n_tp, pieces)),
                 dma((n_tp,)),
-                dma((2, chips, seqs)),
-                dma((chips, seqs)),
+                dma((2, chips, pieces)),
+                dma((chips, pieces)),
                 dma((2, chips)),
                 dma((chips,)),
                 dma((seqs, n_sp)),
@@ -418,7 +436,7 @@
                 collective_id=0, has_side_effects=True, vmem_limit_bytes=60 * 1024 * 1024
             ),
             name="retention",
-        )(tokens, fresh, query_weight, key_weight, value_weight, inverse, log_decay)
+        )(tokens, new_token.reshape(seqs, feat), query_weight, key_weight, value_weight, inverse, log_decay)
 
     return jax.shard_map(
         body,

time: 124 us -> 121 us (0.976)
  local copies, waits for them, and re-layouts: 4.7 us -> 2.82 us
    pad x1 -> x0, local copies, waits for them, and re-layouts: 1.29 us -> none  [body(): fresh = jnp.pad(new_token[:, 0], ((0, NEW_ROWS - seqs), (0, 0)))]
where the time goes in v2:
time: 121 us
  Pallas kernels  117 us (97%)
  local copies, waits for them, and re-layouts  2.82 us (2%)
    pallas_call x1, Pallas kernels, body(): pl.pallas_call(functools.partial(kernel, n_sp, n_tp, parts), out_shape=(j...  117 us
    unnamed x2, local copies, waits for them, and re-layouts  2.82 us

profile of v2, /device:TPU:0, one launch (start us, length us, event | category | flops | bytes accessed | tf_op | source)
XLA Modules:
  0.0 120.5 jit_solution(17845041367481463130)
XLA Ops:
  0.6 117.1 %retention.1 = (bf16[3,8,16,64]{3,2,1,0:T(8,128)(2,1)}, bf16[3,512]{1,0:T(4,128)(2,1)}) custom-call(bf16[3,512,512]{2,1,0:T(8,128)(2,1)} %tokens.1, bf16[3,512]{1,0:T(4,128)(2,1)} %bitcast.1, bf16[4096,512]{1,0:T(8,128)(2,1)} %wq_hbm.1, bf16[4096,512]{1,0:T(8,128)(2,1)} %wk_hbm.1, bf16[4096,512]{1,0:T(8,128)(2,1)} %wv_hbm.1, ...), custom_call_target="tpu_custom_call" | custom-call | tf_op jit(solution)/shard_map/retention/pallas_call | solution.py:398
  117.7 1.5 %copy.11 = bf16[3,8,16,64]{3,2,1,0:T(8,128)(2,1)} copy(bf16[3,8,16,64]{3,2,1,0:T(8,128)(2,1)} %get-tuple-element.4) | data formatting | bytes 98304
  119.3 1.3 %copy.12 = bf16[3,512]{1,0:T(4,128)(2,1)} copy(bf16[3,512]{1,0:T(4,128)(2,1)} %get-tuple-element.5) | data formatting | bytes 6144
